TPU v7x, 512 devices: a whole 4x4x16 slice. The times are simulated.
512 devices in a mesh: sp: 16 (over z), dp: 32 (over y, x, core).
Axes of the slice: x: 4, y: 4, z: 16, core: 2. Of those that a mesh axis runs over, the one named last changes fastest.
Arguments:
- cotangent: bfloat16 [32, 2048, 2048], P('dp', 'sp'), may hold values from -6 to 6
- unit_pre: bfloat16 [32, 2048, 2048], P('dp', None, 'sp'), may hold values from -6 to 6
- gate_pre: bfloat16 [32, 2048, 2048], P('dp', None, 'sp'), may hold values from -15 to 15
- out_weight: bfloat16 [2048, 2048], P('dp', 'sp'), may hold values from -0.125 to 0.125
- mix_weight: bfloat16 [8, 128, 128], replicated, may hold values from -0.5 to 0.5
- mix_bias: bfloat16 [8, 128], replicated, may hold values from 0.099609375 to 1.8984375
- norm_gain: bfloat16 [2048], P('sp'), may hold values from 0.099609375 to 1.8984375
- norm_shift: bfloat16 [2048], P('sp'), may hold values from -3 to 3
Outputs:
- unit_grad: bfloat16 [32, 2048, 2048], P('dp', None, 'sp')
- gate_grad: bfloat16 [32, 2048, 2048], P('dp', None, 'sp')
- out_weight_grad: float32 [2048, 2048], P('dp', 'sp')
- mix_weight_grad: float32 [8, 128, 128], replicated
- mix_bias_grad: float32 [8, 128], replicated
- gain_grad: float32 [2048], P('sp')
- shift_grad: float32 [2048], P('sp')
All inputs are finite; a program needn't handle non-finite values.
Results may differ from a plain program's by a relative error of at most 0.015.
Values may be sent and summed in bfloat16 or wider, within the bound.
A program may use at most 64 MiB of HBM per device.

v0:
```python
import math
import jax
import jax.numpy as jnp
from jax import lax
from jax.sharding import PartitionSpec as P

GW = 2048
GROUPS = 8
BLK = 128
epsilon = 1e-05
tanh_coef = math.sqrt(2.0 / math.pi)


def sum_over(x, axis):
    devices = lax.axis_size(axis)
    copies = jnp.broadcast_to(x[None], (devices, *x.shape))
    return lax.all_to_all(copies, axis, 0, 0, tiled=True).sum(axis=0)


def gelu_slope(values):
    inner = tanh_coef * (values + 0.044715 * values * values * values)
    hyper = jnp.tanh(inner)
    return 0.5 * (1.0 + hyper) + 0.5 * values * (1.0 - hyper * hyper) * tanh_coef * (
        1.0 + 3.0 * 0.044715 * values * values
    )


def local(cotangent, unit_pre, gate_pre, out_weight, mix_weight, mix_bias, norm_gain, norm_shift):
    seq_len = unit_pre.shape[1]
    channels = unit_pre.shape[2]
    group_dim = GW // GROUPS
    blocks = seq_len // BLK
    sp_size = lax.axis_size("sp")
    sp_at = lax.axis_index("sp")
    group = sp_at * channels // group_dim
    weight_rows = lax.all_gather(out_weight, "sp", axis=1, tiled=True)
    weight_whole = lax.all_gather(weight_rows, "dp", axis=0, tiled=True)
    units = unit_pre[0].astype(jnp.float32)
    gates = gate_pre[0].astype(jnp.float32)
    unit_act = jax.nn.gelu(units)
    gate_act = jax.nn.gelu(gates)
    moments = sum_over(
        jnp.stack([jnp.sum(gate_act, axis=-1), jnp.sum(gate_act * gate_act, axis=-1)]), "sp"
    )
    mean_val = moments[0] / GW
    var_val = moments[1] / GW - mean_val * mean_val
    rstd_val = lax.rsqrt(var_val + epsilon)
    centred = (gate_act - mean_val[:, None]) * rstd_val[:, None]
    gain_vec = norm_gain.astype(jnp.float32)
    normed = (centred * gain_vec + norm_shift.astype(jnp.float32)).astype(jnp.bfloat16)
    causal = jnp.arange(BLK)[:, None] >= jnp.arange(BLK)[None, :]
    local_weight = lax.dynamic_index_in_dim(mix_weight, group, 0, keepdims=False)
    masked = jnp.where(causal, local_weight, jnp.zeros_like(local_weight))
    local_bias = lax.dynamic_index_in_dim(mix_bias, group, 0, keepdims=False).astype(jnp.float32)
    normed_blocks = normed.reshape(blocks, BLK, channels)
    mixed = jnp.einsum("ts,nsd->ntd", masked, normed_blocks, preferred_element_type=jnp.float32)
    mixed = (mixed + local_bias[None, :, None]).reshape(seq_len, channels)
    gated = (unit_act * mixed).astype(jnp.bfloat16)
    gated_rows = lax.all_to_all(gated, "sp", split_axis=0, concat_axis=1, tiled=True)
    head_rows = jnp.dot(cotangent[0], weight_whole, preferred_element_type=jnp.float32)
    head = lax.all_to_all(
        head_rows.astype(jnp.bfloat16), "sp", split_axis=1, concat_axis=0, tiled=True
    ).astype(jnp.float32)
    weight_part = lax.dot_general(
        cotangent[0], gated_rows, (((0,), (0,)), ((), ())), preferred_element_type=jnp.float32
    ).astype(jnp.bfloat16)
    token_count = lax.axis_size("dp") * seq_len
    norm_scale = 1.0 / math.sqrt(token_count)
    mix_scale = 1.0 / math.sqrt(token_count // BLK * group_dim)
    plane_sum = lax.psum_scatter(weight_part, "dp", scatter_dimension=0, tiled=True)
    plane_parts = jnp.moveaxis(plane_sum.reshape(plane_sum.shape[0], sp_size, channels), 1, 0)
    arrived = lax.all_to_all(plane_parts, "sp", split_axis=0, concat_axis=0, tiled=True)
    out_grad = arrived.astype(jnp.float32).sum(axis=0) * norm_scale
    unit_grad = (head * mixed * gelu_slope(units)).astype(jnp.bfloat16)
    mix_grad = head * unit_act
    mix_round = mix_grad.astype(jnp.bfloat16).reshape(blocks, BLK, channels)
    mix_term = jnp.einsum(
        "ntd,nsd->ts", mix_round, normed_blocks, preferred_element_type=jnp.float32
    )
    mix_term = jnp.where(causal, mix_term, jnp.float32(0.0))
    bias_term = jnp.sum(mix_grad.reshape(blocks, BLK, channels), axis=(0, 2))
    normed_grad = jnp.einsum(
        "ts,ntd->nsd", masked, mix_round, preferred_element_type=jnp.float32
    ).reshape(seq_len, channels)
    gain_term = jnp.sum(normed_grad * centred, axis=0)
    shift_term = jnp.sum(normed_grad, axis=0)
    scaled = normed_grad * gain_vec
    back_sums = sum_over(
        jnp.stack([jnp.sum(scaled, axis=-1), jnp.sum(scaled * centred, axis=-1)]), "sp"
    )
    first_m = back_sums[0] / GW
    second_m = back_sums[1] / GW
    gate_grad = (
        rstd_val[:, None]
        * (scaled - first_m[:, None] - centred * second_m[:, None])
        * gelu_slope(gates)
    ).astype(jnp.bfloat16)
    group_hot = (jnp.arange(GROUPS) == group).astype(jnp.float32)
    own_hot = (jnp.arange(sp_size) == sp_at).astype(jnp.float32)
    packed = jnp.concatenate(
        [
            (group_hot[:, None, None] * mix_term).reshape(GROUPS * BLK, BLK),
            group_hot[:, None] * bias_term,
            own_hot[:, None] * gain_term,
            own_hot[:, None] * shift_term,
        ]
    )
    total = lax.psum(packed, ("sp", "dp"))
    top = GROUPS * BLK
    weight_total = total[:top].reshape(GROUPS, BLK, BLK)
    bias_total = total[top : top + GROUPS]
    tail = total[top + GROUPS :]
    gain_total = lax.dynamic_index_in_dim(tail, sp_at, 0, keepdims=False)
    shift_total = lax.dynamic_index_in_dim(tail, sp_size + sp_at, 0, keepdims=False)
    return (
        unit_grad[None],
        gate_grad[None],
        out_grad,
        weight_total * mix_scale,
        bias_total * mix_scale,
        gain_total * norm_scale,
        shift_total * norm_scale,
    )


def solution(mesh):
    return jax.shard_map(
        local,
        mesh=mesh,
        in_specs=(
            P("dp", "sp", None),
            P("dp", None, "sp"),
            P("dp", None, "sp"),
            P("dp", "sp"),
            P(),
            P(),
            P("sp"),
            P("sp"),
        ),
        out_specs=(
            P("dp", None, "sp"),
            P("dp", None, "sp"),
            P("dp", "sp"),
            P(),
            P(),
            P("sp"),
            P("sp"),
        ),
        check_vma=False,
    )
```

profile of v0, /device:TPU:32, one launch (start us, length us, event | category | flops | bytes accessed | tf_op | source)
XLA Modules:
  0.0 828.7 jit_solution(9951408123859522207)
XLA Ops:
  7.2 37.3 %all_gather.6 = bf16[64,2048]{1,0:T(8,128)(2,1)} all-gather(bf16[64,128]{1,0:T(8,128)(2,1)} %param.11), channel_id=1, replica_groups=mesh['sp'=16,'dp'=32] {'sp'}, dimensions={1}, use_global_device_ids=true | all-gather | bytes 278528 | tf_op jit(solution)/shard_map/all_gather | solution.py:36
  44.6 1.8 fusion.58
  47.2 8.9 %all-to-all-start.1 = ((f32[16,2,2048]{2,1,0:T(2,128)}), f32[16,2,2048]{2,1,0:T(2,128)S(1)}, u32[]{:S(2)}, u32[]{:S(2)}) async-start(f32[16,2,2048]{2,1,0:T(2,128)} %broadcast_in_dim.11), calls=%async_computation.1 | async-start | bytes 524288 | tf_op jit(solution)/shard_map/all_to_all | solution.py:17
  56.1 54.5 %all-gather.2.cloned.1.call-done = bf16[2048,2048]{1,0:T(8,128)(2,1)} async-done(((bf16[64,2048]{1,0:T(8,128)(2,1)}), bf16[2048,2048]{1,0:T(8,128)(2,1)}) %all-gather.2.cloned.1.call-update) | async-done | bytes 8388624 | tf_op jit(solution)/shard_map/all_gather | solution.py:37
  110.6 4.6 fusion.5
  116.2 12.7 %all-to-all-start = ((bf16[128,16,128]{2,0,1:T(8,128)(2,1)}), bf16[128,16,128]{2,0,1:T(8,128)(2,1)S(1)}, u32[]{:S(2)}, u32[]{:S(2)}) async-start(bf16[128,16,128]{2,0,1:T(8,128)(2,1)} %bitcast.135), calls=%async_computation | async-start | bytes 1048576 | tf_op jit(solution)/shard_map/all_to_all | solution.py:61
  129.0 29.5 %all-to-all-done = bf16[128,16,128]{2,0,1:T(8,128)(2,1)S(1)} async-done(((bf16[128,16,128]{2,0,1:T(8,128)(2,1)}), bf16[128,16,128]{2,0,1:T(8,128)(2,1)S(1)}, u32[]{:S(2)}, u32[]{:S(2)}) %all-to-all-start) | async-done | bytes 524320 | tf_op jit(solution)/shard_map/all_to_all | solution.py:61
  160.1 3.3 fusion.56
  164.2 6.1 all-to-all-start.2
  171.0 17.5 %all-to-all-done.2 = f32[16,2,2048]{2,1,0:T(2,128)S(1)} async-done(((f32[16,2,2048]{2,1,0:T(2,128)}), f32[16,2,2048]{2,1,0:T(2,128)S(1)}, u32[]{:S(2)}, u32[]{:S(2)}) %all-to-all-start.2) | async-done | bytes 262176 | tf_op jit(solution)/shard_map/all_to_all | solution.py:17
  188.7 2.8 fusion.51
  191.5 3.0 multiply_convert_fusion
  194.4 6.1 all-to-all-start.3
  200.9 2.5 fusion.6
  204.6 24.2 %all-to-all-done.3 = bf16[16,128,128]{2,1,0:T(8,128)(2,1)S(1)} async-done(((bf16[16,128,128]{2,1,0:T(8,128)(2,1)}), bf16[16,128,128]{2,1,0:T(8,128)(2,1)S(1)}, u32[]{:S(2)}, u32[]{:S(2)}) %all-to-all-start.3) | async-done | bytes 524320 | tf_op jit(solution)/shard_map/all_to_all | solution.py:59
  229.2 5.5 convert_bitcast_fusion
  234.7 12.4 %copy.42 = bf16[2048,2048]{1,0:T(8,128)(2,1)} copy(bf16[2048,2048]{0,1:T(8,128)(2,1)} %convert_bitcast_fusion) | data formatting | bytes 16777216
  247.1 423.4 %all-reduce.2.cloned.1.call-done = f32[1064,128]{1,0:T(8,128)} async-done(((f32[1064,128]{1,0:T(8,128)}), f32[1064,128]{1,0:T(8,128)}) %all-reduce.2.cloned.1.call-update) | async-done | bytes 544784 | tf_op jit(solution)/shard_map/psum | solution.py:108
  671.2 117.9 %reduce-scatter.4.cloned.1.call-done = bf16[64,2048]{1,0:T(8,128)(2,1)} async-done(((bf16[2048,2048]{1,0:T(8,128)(2,1)}), bf16[64,2048]{1,0:T(8,128)(2,1)}) %reduce-scatter.4.cloned.1.call-update) | async-done | bytes 262160
  791.3 12.7 %all-to-all-start.4 = ((bf16[16,64,128]{2,1,0:T(8,128)(2,1)}), bf16[16,64,128]{2,1,0:T(8,128)(2,1)S(1)}, u32[]{:S(2)}, u32[]{:S(2)}) async-start(bf16[16,64,128]{2,1,0:T(8,128)(2,1)} %bitcast.29), calls=%async_computation.4 | async-start | bytes 524288 | tf_op jit(solution)/shard_map/all_to_all | solution.py:72
  804.5 1.3 slice_multiply_fusion.5
  805.7 1.9 slice_multiply_fusion
  807.6 1.5 fusion.30
  809.1 12.2 %all-to-all-done.4 = bf16[16,64,128]{2,1,0:T(8,128)(2,1)S(1)} async-done(((bf16[16,64,128]{2,1,0:T(8,128)(2,1)}), bf16[16,64,128]{2,1,0:T(8,128)(2,1)S(1)}, u32[]{:S(2)}, u32[]{:S(2)}) %all-to-all-start.4) | async-done | bytes 262176 | tf_op jit(solution)/shard_map/all_to_all | solution.py:72
  (52 shorter events, 11.2 us)
Async XLA Ops:
  7.2 103.5 %copy-start = (bf16[1,128,2048]{2,1,0:T(8,128)(2,1)S(1)}, bf16[1,128,2048]{2,1,0:T(8,128)(2,1)}, u32[]{:S(2)}) copy-start(bf16[1,128,2048]{2,1,0:T(8,128)(2,1)} %param.8) | copy-start | bytes 1572868
  7.2 103.4 %all-gather.2.cloned.1.call-start = ((), (), s32[]{:S(2)}) async-start(), calls=%async_computation.6 | async-start | bytes 8650752 | tf_op jit(solution)/shard_map/all_gather | solution.py:37
  47.2 69.0 %all-to-all-start.1 = ((f32[16,2,2048]{2,1,0:T(2,128)}), f32[16,2,2048]{2,1,0:T(2,128)S(1)}, u32[]{:S(2)}, u32[]{:S(2)}) async-start(f32[16,2,2048]{2,1,0:T(2,128)} %broadcast_in_dim.11), calls=%async_computation.1 | async-start | bytes 524288 | tf_op jit(solution)/shard_map/all_to_all | solution.py:17
  56.1 72.8 %copy-start.5 = (bf16[128]{0:T(256)(128)(2,1)S(1)}, bf16[128]{0:T(256)(128)(2,1)}, u32[]{:S(2)}) copy-start(bf16[128]{0:T(256)(128)(2,1)} %param.14) | copy-start | bytes 772
  56.1 102.5 %copy-start.2 = (bf16[1,2048,128]{2,1,0:T(8,128)(2,1)S(1)}, bf16[1,2048,128]{2,1,0:T(8,128)(2,1)}, u32[]{:S(2)}) copy-start(bf16[1,2048,128]{2,1,0:T(8,128)(2,1)} %param.9) | copy-start | bytes 1572868
  56.1 104.0 %copy-start.1 = (bf16[1,2048,128]{2,1,0:T(8,128)(2,1)S(1)}, bf16[1,2048,128]{2,1,0:T(8,128)(2,1)}, u32[]{:S(2)}) copy-start(bf16[1,2048,128]{2,1,0:T(8,128)(2,1)} %param.10) | copy-start | bytes 1572868
  115.3 55.1 %copy-start.6 = (bf16[128]{0:T(256)(128)(2,1)S(1)}, bf16[128]{0:T(256)(128)(2,1)}, u32[]{:S(2)}) copy-start(bf16[128]{0:T(256)(128)(2,1)} %param.15) | copy-start | bytes 772
  116.2 42.4 %all-to-all-start = ((bf16[128,16,128]{2,0,1:T(8,128)(2,1)}), bf16[128,16,128]{2,0,1:T(8,128)(2,1)S(1)}, u32[]{:S(2)}, u32[]{:S(2)}) async-start(bf16[128,16,128]{2,0,1:T(8,128)(2,1)} %bitcast.135), calls=%async_computation | async-start | bytes 1048576 | tf_op jit(solution)/shard_map/all_to_all | solution.py:61
  159.1 1.0 copy-start.3
  164.2 24.4 %all-to-all-start.2 = ((f32[16,2,2048]{2,1,0:T(2,128)}), f32[16,2,2048]{2,1,0:T(2,128)S(1)}, u32[]{:S(2)}, u32[]{:S(2)}) async-start(f32[16,2,2048]{2,1,0:T(2,128)} %broadcast_in_dim.15), calls=%async_computation.2 | async-start | bytes 524288 | tf_op jit(solution)/shard_map/all_to_all | solution.py:17
  194.4 34.5 %all-to-all-start.3 = ((bf16[16,128,128]{2,1,0:T(8,128)(2,1)}), bf16[16,128,128]{2,1,0:T(8,128)(2,1)S(1)}, u32[]{:S(2)}, u32[]{:S(2)}) async-start(bf16[16,128,128]{2,1,0:T(8,128)(2,1)} %get-tuple-element.36), calls=%async_computation.3 | async-start | bytes 1048576 | tf_op jit(solution)/shard_map/all_to_all | solution.py:59
  200.5 470.0 %all-reduce.2.cloned.1.call-start = ((), (), s32[]{:S(2)}) async-start(), calls=%async_computation.7 | async-start | bytes 1089536 | tf_op jit(solution)/shard_map/psum | solution.py:108
  204.6 584.5 %reduce-scatter.4.cloned.1.call-start = ((), (), s32[]{:S(2)}) async-start(), calls=%async_computation.8 | async-start | bytes 8650752
  247.1 560.5 %copy-start.4 = (f32[16,128,128]{2,1,0:T(8,128)S(1)}, f32[16,128,128]{2,1,0:T(8,128)}, u32[]{:S(2)}) copy-start(f32[16,128,128]{2,1,0:T(8,128)} %get-tuple-element.37) | copy-start | bytes 3145732
  791.3 30.0 %all-to-all-start.4 = ((bf16[16,64,128]{2,1,0:T(8,128)(2,1)}), bf16[16,64,128]{2,1,0:T(8,128)(2,1)S(1)}, u32[]{:S(2)}, u32[]{:S(2)}) async-start(bf16[16,64,128]{2,1,0:T(8,128)(2,1)} %bitcast.29), calls=%async_computation.4 | async-start | bytes 524288 | tf_op jit(solution)/shard_map/all_to_all | solution.py:72
Sparse Core Ops, SparseCore 0:
  44.7 65.8 all-gather.1
  206.8 463.6 all-reduce.1
  675.1 114.0 reduce-scatter.3
where the time goes:
time: 830 us; the launch traced here: 829 us
  waiting for transfers between devices  679 us (82%)
  starting transfers between devices  46.6 us (6%)
  blocking collectives  37.3 us (4%)
  local copies, waits for them, and re-layouts  19.8 us (2%)
  matrix products  18.9 us (2%)
  between operations  13.9 us (2%)
  other arithmetic  12.7 us (2%)
    psum x1, waiting for transfers between devices, local(): total = lax.psum(packed, ('sp', 'dp'))  423 us
    unnamed x4, waiting for transfers between devices  118 us
    all_gather x1, waiting for transfers between devices, local(): weight_whole = lax.all_gather(weight_rows, 'dp', axis=0, tiled=True)  54.5 us
    all_gather x1, blocking collectives, local(): weight_rows = lax.all_gather(out_weight, 'sp', axis=1, tiled=True)  37.3 us
    all_to_all x1, waiting for transfers between devices, local(): lax.all_to_all(head_rows.astype(jnp.bfloat16), 'sp', split_axis=1, concat...  29.5 us
    all_to_all x1, waiting for transfers between devices, local(): lax.all_to_all(gated, 'sp', split_axis=0, concat_axis=1, tiled=True)  24.2 us
    all_to_all x2, waiting for transfers between devices, sum_over(): return lax.all_to_all(copies, axis, 0, 0, tiled=True).sum(axis=0)  17.5 us
  transfers between devices with their start and end apart: 8, of which 7 were waited for; matrix products, arithmetic and copies ran while one was open for 4% of the time, Pallas kernels for 0%

commit v1 on v0

--- a/solution.py
+++ b/solution.py
@@ -105,7 +105,7 @@
             own_hot[:, None] * shift_term,
         ]
     )
-    total = lax.psum(packed, ("sp", "dp"))
+    total = lax.psum(lax.psum(packed, "dp"), "sp")
     top = GROUPS * BLK
     weight_total = total[:top].reshape(GROUPS, BLK, BLK)
     bias_total = total[top : top + GROUPS]

time: 830 us -> 635 us (0.77)
  waiting for transfers between devices: 679 us -> 484 us
    psum x1 -> x2, waiting for transfers between devices: 423 us -> 254 us  [local(): total = lax.psum(lax.psum(packed, 'dp'), 'sp')]
    all_to_all x1, waiting for transfers between devices: 24.2 us -> 0.01 us  [local(): lax.all_to_all(gated, 'sp', split_axis=0, concat_axis=1, tiled=True)]
    unnamed x4 -> x5, waiting for transfers between devices: 118 us -> 116 us
  transfers between devices with their start and end apart: 8 -> 9, of which waited for: 7 -> 7; matrix products, arithmetic and copies ran while one was open for 4% -> 6% of each run, Pallas kernels for 0% -> 0%
where the time goes in v1:
time: 635 us; the launch traced here: 633 us
  waiting for transfers between devices  484 us (76%)
  starting transfers between devices  46.6 us (7%)
  blocking collectives  37.3 us (6%)
  local copies, waits for them, and re-layouts  19.8 us (3%)
  matrix products  19 us (3%)
  between operations  13.9 us (2%)
  other arithmetic  12.7 us (2%)
    psum x2, waiting for transfers between devices, local(): total = lax.psum(lax.psum(packed, 'dp'), 'sp')  254 us
    unnamed x5, waiting for transfers between devices  116 us
    all_gather x1, waiting for transfers between devices, local(): weight_whole = lax.all_gather(weight_rows, 'dp', axis=0, tiled=True)  54.5 us
    all_gather x1, blocking collectives, local(): weight_rows = lax.all_gather(out_weight, 'sp', axis=1, tiled=True)  37.3 us
    all_to_all x1, waiting for transfers between devices, local(): lax.all_to_all(head_rows.astype(jnp.bfloat16), 'sp', split_axis=1, concat...  29.5 us
    all_to_all x2, waiting for transfers between devices, sum_over(): return lax.all_to_all(copies, axis, 0, 0, tiled=True).sum(axis=0)  17.5 us
    unnamed x18, local copies, waits for them, and re-layouts  15.4 us
    all_to_all x2, starting transfers between devices, sum_over(): return lax.all_to_all(copies, axis, 0, 0, tiled=True).sum(axis=0)  15 us
  transfers between devices with their start and end apart: 9, of which 7 were waited for; matrix products, arithmetic and copies ran while one was open for 6% of the time, Pallas kernels for 0%

profile of v1, /device:TPU:32, one launch (start us, length us, event | category | flops | bytes accessed | tf_op | source)
XLA Modules:
  0.0 633.3 jit_solution(16026258284083626327)
XLA Ops:
  7.2 37.3 %all_gather.6 = bf16[64,2048]{1,0:T(8,128)(2,1)} all-gather(bf16[64,128]{1,0:T(8,128)(2,1)} %param.11), channel_id=1, replica_groups=mesh['sp'=16,'dp'=32] {'sp'}, dimensions={1}, use_global_device_ids=true | all-gather | bytes 278528 | tf_op jit(solution)/shard_map/all_gather | solution.py:36
  44.6 1.8 fusion.58
  47.2 8.9 %all-to-all-start.1 = ((f32[16,2,2048]{2,1,0:T(2,128)}), f32[16,2,2048]{2,1,0:T(2,128)S(1)}, u32[]{:S(2)}, u32[]{:S(2)}) async-start(f32[16,2,2048]{2,1,0:T(2,128)} %broadcast_in_dim.11), calls=%async_computation.1 | async-start | bytes 524288 | tf_op jit(solution)/shard_map/all_to_all | solution.py:17
  56.1 54.5 %all-gather.2.cloned.1.call-done = bf16[2048,2048]{1,0:T(8,128)(2,1)} async-done(((bf16[64,2048]{1,0:T(8,128)(2,1)}), bf16[2048,2048]{1,0:T(8,128)(2,1)}) %all-gather.2.cloned.1.call-update) | async-done | bytes 8388624 | tf_op jit(solution)/shard_map/all_gather | solution.py:37
  110.6 4.6 fusion.5
  116.2 12.7 %all-to-all-start = ((bf16[128,16,128]{2,0,1:T(8,128)(2,1)}), bf16[128,16,128]{2,0,1:T(8,128)(2,1)S(1)}, u32[]{:S(2)}, u32[]{:S(2)}) async-start(bf16[128,16,128]{2,0,1:T(8,128)(2,1)} %bitcast.135), calls=%async_computation | async-start | bytes 1048576 | tf_op jit(solution)/shard_map/all_to_all | solution.py:61
  129.0 29.5 %all-to-all-done = bf16[128,16,128]{2,0,1:T(8,128)(2,1)S(1)} async-done(((bf16[128,16,128]{2,0,1:T(8,128)(2,1)}), bf16[128,16,128]{2,0,1:T(8,128)(2,1)S(1)}, u32[]{:S(2)}, u32[]{:S(2)}) %all-to-all-start) | async-done | bytes 524320 | tf_op jit(solution)/shard_map/all_to_all | solution.py:61
  160.1 3.3 fusion.56
  164.2 6.1 all-to-all-start.2
  171.0 17.5 %all-to-all-done.2 = f32[16,2,2048]{2,1,0:T(2,128)S(1)} async-done(((f32[16,2,2048]{2,1,0:T(2,128)}), f32[16,2,2048]{2,1,0:T(2,128)S(1)}, u32[]{:S(2)}, u32[]{:S(2)}) %all-to-all-start.2) | async-done | bytes 262176 | tf_op jit(solution)/shard_map/all_to_all | solution.py:17
  188.7 2.8 fusion.51
  191.5 3.0 multiply_convert_fusion
  194.4 6.1 all-to-all-start.3
  200.9 2.5 fusion.6
  204.7 132.2 %all-reduce.3.cloned.1.call-done = f32[1064,128]{1,0:T(8,128)} async-done(((f32[1064,128]{1,0:T(8,128)}), f32[1064,128]{1,0:T(8,128)}) %all-reduce.3.cloned.1.call-update) | async-done | bytes 544784 | tf_op jit(solution)/shard_map/psum | solution.py:108
  337.3 5.5 convert_bitcast_fusion
  342.8 12.3 %copy.42 = bf16[2048,2048]{1,0:T(8,128)(2,1)} copy(bf16[2048,2048]{0,1:T(8,128)(2,1)} %convert_bitcast_fusion) | data formatting | bytes 16777216
  355.2 121.6 %all-reduce.5.cloned.1.call-done = f32[1064,128]{1,0:T(8,128)} async-done(((f32[1064,128]{1,0:T(8,128)}), f32[1064,128]{1,0:T(8,128)}) %all-reduce.5.cloned.1.call-update) | async-done | bytes 544784 | tf_op jit(solution)/shard_map/psum | solution.py:108
  477.5 116.3 %reduce-scatter.4.cloned.1.call-done = bf16[64,2048]{1,0:T(8,128)(2,1)} async-done(((bf16[2048,2048]{1,0:T(8,128)(2,1)}), bf16[64,2048]{1,0:T(8,128)(2,1)}) %reduce-scatter.4.cloned.1.call-update) | async-done | bytes 262160
  595.9 12.7 %all-to-all-start.4 = ((bf16[16,64,128]{2,1,0:T(8,128)(2,1)}), bf16[16,64,128]{2,1,0:T(8,128)(2,1)S(1)}, u32[]{:S(2)}, u32[]{:S(2)}) async-start(bf16[16,64,128]{2,1,0:T(8,128)(2,1)} %bitcast.29), calls=%async_computation.4 | async-start | bytes 524288 | tf_op jit(solution)/shard_map/all_to_all | solution.py:72
  609.0 1.3 slice_multiply_fusion.5
  610.3 1.9 slice_multiply_fusion
  612.2 1.5 fusion.30
  613.7 12.2 %all-to-all-done.4 = bf16[16,64,128]{2,1,0:T(8,128)(2,1)S(1)} async-done(((bf16[16,64,128]{2,1,0:T(8,128)(2,1)}), bf16[16,64,128]{2,1,0:T(8,128)(2,1)S(1)}, u32[]{:S(2)}, u32[]{:S(2)}) %all-to-all-start.4) | async-done | bytes 262176 | tf_op jit(solution)/shard_map/all_to_all | solution.py:72
  (55 shorter events, 11.2 us)
Async XLA Ops:
  7.2 103.5 %copy-start = (bf16[1,128,2048]{2,1,0:T(8,128)(2,1)S(1)}, bf16[1,128,2048]{2,1,0:T(8,128)(2,1)}, u32[]{:S(2)}) copy-start(bf16[1,128,2048]{2,1,0:T(8,128)(2,1)} %param.8) | copy-start | bytes 1572868
  7.2 103.4 %all-gather.2.cloned.1.call-start = ((), (), s32[]{:S(2)}) async-start(), calls=%async_computation.6 | async-start | bytes 8650752 | tf_op jit(solution)/shard_map/all_gather | solution.py:37
  47.2 69.0 %all-to-all-start.1 = ((f32[16,2,2048]{2,1,0:T(2,128)}), f32[16,2,2048]{2,1,0:T(2,128)S(1)}, u32[]{:S(2)}, u32[]{:S(2)}) async-start(f32[16,2,2048]{2,1,0:T(2,128)} %broadcast_in_dim.11), calls=%async_computation.1 | async-start | bytes 524288 | tf_op jit(solution)/shard_map/all_to_all | solution.py:17
  56.1 72.8 %copy-start.5 = (bf16[128]{0:T(256)(128)(2,1)S(1)}, bf16[128]{0:T(256)(128)(2,1)}, u32[]{:S(2)}) copy-start(bf16[128]{0:T(256)(128)(2,1)} %param.14) | copy-start | bytes 772
  56.1 102.5 %copy-start.2 = (bf16[1,2048,128]{2,1,0:T(8,128)(2,1)S(1)}, bf16[1,2048,128]{2,1,0:T(8,128)(2,1)}, u32[]{:S(2)}) copy-start(bf16[1,2048,128]{2,1,0:T(8,128)(2,1)} %param.9) | copy-start | bytes 1572868
  56.1 104.0 %copy-start.1 = (bf16[1,2048,128]{2,1,0:T(8,128)(2,1)S(1)}, bf16[1,2048,128]{2,1,0:T(8,128)(2,1)}, u32[]{:S(2)}) copy-start(bf16[1,2048,128]{2,1,0:T(8,128)(2,1)} %param.10) | copy-start | bytes 1572868
  115.3 55.1 %copy-start.6 = (bf16[128]{0:T(256)(128)(2,1)S(1)}, bf16[128]{0:T(256)(128)(2,1)}, u32[]{:S(2)}) copy-start(bf16[128]{0:T(256)(128)(2,1)} %param.15) | copy-start | bytes 772
  116.2 42.4 %all-to-all-start = ((bf16[128,16,128]{2,0,1:T(8,128)(2,1)}), bf16[128,16,128]{2,0,1:T(8,128)(2,1)S(1)}, u32[]{:S(2)}, u32[]{:S(2)}) async-start(bf16[128,16,128]{2,0,1:T(8,128)(2,1)} %bitcast.135), calls=%async_computation | async-start | bytes 1048576 | tf_op jit(solution)/shard_map/all_to_all | solution.py:61
  159.1 1.0 copy-start.3
  164.2 24.4 %all-to-all-start.2 = ((f32[16,2,2048]{2,1,0:T(2,128)}), f32[16,2,2048]{2,1,0:T(2,128)S(1)}, u32[]{:S(2)}, u32[]{:S(2)}) async-start(f32[16,2,2048]{2,1,0:T(2,128)} %broadcast_in_dim.15), calls=%async_computation.2 | async-start | bytes 524288 | tf_op jit(solution)/shard_map/all_to_all | solution.py:17
  194.4 142.6 %all-to-all-start.3 = ((bf16[16,128,128]{2,1,0:T(8,128)(2,1)}), bf16[16,128,128]{2,1,0:T(8,128)(2,1)S(1)}, u32[]{:S(2)}, u32[]{:S(2)}) async-start(bf16[16,128,128]{2,1,0:T(8,128)(2,1)} %get-tuple-element.36), calls=%async_computation.3 | async-start | bytes 1048576 | tf_op jit(solution)/shard_map/all_to_all | solution.py:59
  200.5 136.4 %all-reduce.3.cloned.1.call-start = ((), (), s32[]{:S(2)}) async-start(), calls=%async_computation.7 | async-start | bytes 1089536 | tf_op jit(solution)/shard_map/psum | solution.py:108
  204.6 272.2 %all-reduce.5.cloned.1.call-start = ((), (), s32[]{:S(2)}) async-start(), calls=%async_computation.8 | async-start | bytes 1089536 | tf_op jit(solution)/shard_map/psum | solution.py:108
  336.9 256.8 %reduce-scatter.4.cloned.1.call-start = ((), (), s32[]{:S(2)}) async-start(), calls=%async_computation.9 | async-start | bytes 8650752
  355.2 257.0 %copy-start.4 = (f32[16,128,128]{2,1,0:T(8,128)S(1)}, f32[16,128,128]{2,1,0:T(8,128)}, u32[]{:S(2)}) copy-start(f32[16,128,128]{2,1,0:T(8,128)} %get-tuple-element.37) | copy-start | bytes 3145732
  595.9 30.0 %all-to-all-start.4 = ((bf16[16,64,128]{2,1,0:T(8,128)(2,1)}), bf16[16,64,128]{2,1,0:T(8,128)(2,1)S(1)}, u32[]{:S(2)}, u32[]{:S(2)}) async-start(bf16[16,64,128]{2,1,0:T(8,128)(2,1)} %bitcast.29), calls=%async_computation.4 | async-start | bytes 524288 | tf_op jit(solution)/shard_map/all_to_all | solution.py:72
Sparse Core Ops, SparseCore 0:
  44.7 65.8 all-gather.1
  204.7 132.1 all-reduce.2
  339.2 137.4 all-reduce.4
  481.2 112.4 reduce-scatter.3
